TPU v7x, 256 devices: a 4x2x16 block of a 4x16x16 slice. The times are simulated.
256 devices in a mesh: grp: 2 (over y), sp: 32 (over z, core), tp: 4 (over x).
Axes of the slice: x: 4, y: 2, z: 16, core: 2. Of those that a mesh axis runs over, the one named last changes fastest.
The devices are a block of a 4x16x16 slice.
Arguments:
- hidden_in: bfloat16 [16384, 2048], P(('grp', 'sp')), parts along dimension 0, may hold values from -6 to 6
- query_latent_rows: bfloat16 [16384, 768], P(('grp', 'sp')), parts along dimension 0, may hold values from -6 to 6
- key_value_latent: bfloat16 [16384, 512], P(('grp', 'sp')), parts along dimension 0, may hold values from -6 to 6
- rotary_key: bfloat16 [16384, 32], P(('grp', 'sp')), parts along dimension 0, may hold values from -64 to 64
- query_norm_gain: float32 [768], replicated, may hold values from 0.1 to 1.9
- key_value_gain: float32 [512], replicated, may hold values from 0.1 to 1.9
- query_up_weight: bfloat16 [768, 1536], P(None, 'tp'), may hold values from -0.625 to 0.625
- key_value_up_weight: bfloat16 [512, 2048], P(None, 'tp'), may hold values from -0.25 to 0.25
- out_proj: bfloat16 [1024, 2048], P('tp'), may hold values from -0.1875 to 0.1875
- feed_gain: float32 [2048], replicated, may hold values from 0.1 to 1.9
- feed_up: bfloat16 [2048, 8192], P('sp', 'tp'), may hold values from -0.125 to 0.125
- feed_down: bfloat16 [8192, 2048], P('tp', 'sp'), may hold values from -0.0625 to 0.0625
Outputs:
- layer_out: bfloat16 [16384, 2048], P(('grp', 'sp', 'tp')), parts along dimension 0
There are 2 independent parts, one for each index of `grp`. A program takes and returns all parts, laid end to end along the dimension named above; an argument that names none is the same for every part. Nothing has to cross between parts.
All inputs are finite; a program needn't handle non-finite values.
Results may differ from a plain program's by a relative error of at most 0.02.
Values may be sent and summed in bfloat16 or wider, within the bound.
A program may use at most 128 MiB of HBM per device.

v0:
```python
import math
import jax
import jax.numpy as jnp
from jax import lax
from jax.sharding import PartitionSpec as P

QUERY_KEY_PLAIN = 64
QUERY_KEY_ROTARY = 32
VALUE_HEAD_SIZE = 64


def cut_along(value, dim, count):
    before, after = (value.shape[:dim], value.shape[dim + 1 :])
    return jnp.moveaxis(value.reshape(*before, count, -1, *after), dim, 0)


def sum_at_owner(value, axis, dim):
    count = lax.axis_size(axis)
    pieces = lax.all_to_all(cut_along(value, dim, count), axis, 0, 0, tiled=True)
    return jnp.sum(pieces.astype(jnp.float32), axis=0)


def from_everyone(value, axis):
    copies = jnp.broadcast_to(value, (lax.axis_size(axis), *value.shape))
    return lax.all_to_all(copies, axis, split_axis=0, concat_axis=0, tiled=True)


def in_order(pieces, dim):
    lengths = list(pieces.shape[1:])
    lengths[dim] *= pieces.shape[0]
    return jnp.moveaxis(pieces, 0, dim).reshape(lengths)


def gather_directly(value, axis, dim):
    pieces = from_everyone(value, axis)
    return in_order(pieces, dim)


def normalize(values, gain):
    floats = values.astype(jnp.float32)
    return floats * lax.rsqrt(jnp.mean(floats * floats, axis=-1, keepdims=True) + 1e-06) * gain


def rotate(values, position):
    half_size = values.shape[-1] // 2
    inverse = 10000.0 ** (-jnp.arange(half_size, dtype=jnp.float32) * 2.0 / values.shape[-1])
    angles = position[:, None] * inverse[None, :]
    cosine = jnp.concatenate([jnp.cos(angles), jnp.cos(angles)], axis=-1)
    sine = jnp.concatenate([jnp.sin(angles), jnp.sin(angles)], axis=-1)
    shape = (values.shape[0],) + (1,) * (values.ndim - 2) + (values.shape[-1],)
    turned = jnp.concatenate([-values[..., half_size:], values[..., :half_size]], axis=-1)
    return values * cosine.reshape(shape) + turned * sine.reshape(shape)


def on_device(
    hidden_in,
    query_latent_rows,
    key_value_latent,
    rotary_key,
    query_norm_gain,
    key_value_gain,
    query_up_weight,
    key_value_up_weight,
    out_proj,
    feed_gain,
    feed_up,
    feed_down,
):
    tokens_here = hidden_in.shape[0]
    heads_here = query_up_weight.shape[1] // (QUERY_KEY_PLAIN + QUERY_KEY_ROTARY)
    position = (lax.axis_index("sp") * tokens_here + jnp.arange(tokens_here)).astype(jnp.float32)
    scale_factor = (QUERY_KEY_PLAIN + QUERY_KEY_ROTARY) ** (-0.5)
    query_norm = normalize(query_latent_rows, query_norm_gain).astype(jnp.bfloat16)
    queries = jnp.dot(query_norm, query_up_weight, preferred_element_type=jnp.float32).reshape(
        tokens_here, heads_here, QUERY_KEY_PLAIN + QUERY_KEY_ROTARY
    )
    queries = jnp.concatenate(
        [queries[..., :QUERY_KEY_PLAIN], rotate(queries[..., QUERY_KEY_PLAIN:], position)], axis=-1
    ).astype(jnp.bfloat16)
    query_plain = queries[..., :QUERY_KEY_PLAIN]
    query_turned = queries[..., QUERY_KEY_PLAIN:]
    latent = normalize(key_value_latent, key_value_gain).astype(jnp.bfloat16)
    key_rope = rotate(rotary_key.astype(jnp.float32), position).astype(jnp.bfloat16)

    def attend_block(carry, key_plain, value_rows, rope_rows):
        row_max, denom, accum = carry
        scores = jnp.einsum(
            "qhd,khd->hqk", query_plain, key_plain, preferred_element_type=jnp.float32
        )
        scores = scores + jnp.einsum(
            "qhd,kd->hqk", query_turned, rope_rows, preferred_element_type=jnp.float32
        )
        scores = scores * scale_factor
        new_max = jnp.maximum(row_max, jnp.max(scores, axis=-1))
        expo = jnp.exp(scores - new_max[:, :, None])
        factor = jnp.exp(row_max - new_max)
        denom = denom * factor + jnp.sum(expo, axis=-1)
        update = jnp.einsum(
            "hqk,khd->qhd",
            expo.astype(jnp.bfloat16),
            value_rows,
            preferred_element_type=jnp.float32,
        )
        accum = accum * jnp.transpose(factor)[:, :, None] + update
        return (new_max, denom, accum)

    start_carry = (
        jnp.full((heads_here, tokens_here), -1e30, jnp.float32),
        jnp.zeros((heads_here, tokens_here), jnp.float32),
        jnp.zeros((tokens_here, heads_here, VALUE_HEAD_SIZE), jnp.float32),
    )
    own_keys = jnp.dot(latent, key_value_up_weight, preferred_element_type=jnp.float32).astype(
        jnp.bfloat16
    )
    pieces = (
        lax.all_gather(own_keys, "sp", axis=0, tiled=True),
        lax.all_gather(key_rope, "sp", axis=0, tiled=True),
    )
    rows_in = pieces[0].shape[0]
    block = math.gcd(rows_in, 1024)

    def step_block(index, inner):
        first = index * block
        bulk = lax.dynamic_slice_in_dim(pieces[0], first, block, 0)
        rope_rows = lax.dynamic_slice_in_dim(pieces[1], first, block, 0)
        bulk = bulk.reshape(block, heads_here, QUERY_KEY_PLAIN + VALUE_HEAD_SIZE)
        return attend_block(
            inner, bulk[..., :QUERY_KEY_PLAIN], bulk[..., QUERY_KEY_PLAIN:], rope_rows
        )

    final_carry = lax.fori_loop(0, rows_in // block, step_block, start_carry)
    denom = final_carry[1]
    accum = final_carry[2]
    mixed = (
        (accum / jnp.transpose(denom)[:, :, None])
        .astype(jnp.bfloat16)
        .reshape(tokens_here, heads_here * VALUE_HEAD_SIZE)
    )
    share = tokens_here // lax.axis_size("tp")
    lead = lax.axis_index("tp") * share
    branch = sum_at_owner(
        jnp.dot(mixed, out_proj, preferred_element_type=jnp.float32).astype(jnp.bfloat16), "tp", 0
    )
    own_rows = lax.dynamic_slice_in_dim(hidden_in, lead, share, 0)
    middle_own = (own_rows.astype(jnp.float32) + branch).astype(jnp.bfloat16)
    normed = gather_directly(normalize(middle_own, feed_gain).astype(jnp.bfloat16), "tp", 0)
    upward = jnp.dot(
        normed,
        lax.all_gather(feed_up, "sp", axis=0, tiled=True),
        preferred_element_type=jnp.float32,
    )
    activated = jnp.square(jax.nn.relu(upward)).astype(jnp.bfloat16)
    partial_sum = jnp.dot(
        activated,
        lax.all_gather(feed_down, "sp", axis=1, tiled=True),
        preferred_element_type=jnp.float32,
    )
    feed = sum_at_owner(partial_sum.astype(jnp.bfloat16), "tp", 0)
    return (middle_own.astype(jnp.float32) + feed).astype(jnp.bfloat16)


def solution(mesh):
    return jax.shard_map(
        on_device,
        mesh=mesh,
        in_specs=(
            P(("grp", "sp"), None),
            P(("grp", "sp"), None),
            P(("grp", "sp"), None),
            P(("grp", "sp"), None),
            P(),
            P(),
            P(None, "tp"),
            P(None, "tp"),
            P("tp", None),
            P(),
            P("sp", "tp"),
            P("tp", "sp"),
        ),
        out_specs=P(("grp", "sp", "tp"), None),
        check_vma=False,
    )
```

profile of v0, /device:TPU:33, one launch (start us, length us, event | category | flops | bytes accessed | tf_op | source)
XLA Modules:
  0.0 289.8 jit_solution(13299205808065012109)
XLA Ops:
  6.6 1.2 fusion.25
  7.7 2.2 convolution_convert_fusion.2
  13.0 1.2 fusion.22
  14.2 1.6 fusion.32
  16.1 55.3 %all_gather.13 = bf16[8192,32]{0,1:T(8,128)(2,1)} all-gather(bf16[256,32]{0,1:T(8,128)(2,1)S(1)} %get-tuple-element.215), channel_id=1, replica_groups=mesh['grp'=2,'sp'=32,'tp'=4] {'sp'}, dimensions={0}, use_global_device_ids=true | all-gather | bytes 540672 | tf_op jit(solution)/shard_map/all_gather | solution.py:117
  72.0 30.9 %all-gather.4.cloned.1.call-done = bf16[8192,512]{1,0:T(8,128)(2,1)} async-done(((bf16[256,512]{1,0:T(8,128)(2,1)}), bf16[8192,512]{1,0:T(8,128)(2,1)}) %all-gather.4.cloned.1.call-update) | async-done | bytes 8388624 | tf_op jit(solution)/shard_map/all_gather | solution.py:116
  102.9 83.0 %while.18 = (s32[]{:T(128)}, f32[4,256]{1,0:T(4,128)S(1)}, f32[4,256]{1,0:T(4,128)S(1)}, f32[256,4,64]{0,2,1:T(8,128)S(1)}, bf16[8192,512]{1,0:T(8,128)(2,1)}, /...) while((s32[]{:T(128)}, f32[4,256]{1,0:T(4,128)S(1)}, ...), condition=%wide.region_5.0_spmd.clone, body=%wide.region_2.0_spmd.clone.sunk | while | flops 343087104 | bytes 44105964 | solution.py:131
  102.9 1.3 constant_dynamic-slice_fusion.2
  104.8 0.8 fusion.70
  105.6 3.5 %fusion.71 = (f32[4,256]{1,0:T(4,128)S(1)}, f32[4,256,1024]{1,2,0:T(8,128)}) fusion(bf16[256,4,32]{0,2,1:T(8,128)(2,1)S(1)} %copy-done.2, bf16[8192,32]{0,1:T(8,128)(2,1)} %get-tuple-element.307, s32[]{:T(128)S(6)} %select_n.14, f32[4,1024,256]{2,1,0:T(8,128)S(1)} %fusion.70), kind=kOutput, calls=%fused_computation.74.clone.1 | convolution fusion | flops 70253568 | bytes 8523780 | tf_op jit(solution)/shard_map/while/body/eval_jaxpr/qhd,kd->hqk/dot_general | solution.py:90
  109.1 3.1 %fusion.75 = f32[256,4,64]{0,2,1:T(8,128)S(1)} fusion(f32[4,256,1024]{1,2,0:T(8,128)} %get-tuple-element.275, f32[4,256]{1,0:T(4,128)S(1)} %get-tuple-element.302, bf16[1024,4,128]{0,2,1:T(8,128)(2,1)S(1)} %bitcast.46, f32[256,4,64]{0,2,1:T(8,128)S(1)} %get-tuple-element.292, f32[256,4]{0,1:T(4,128)S(1)} %get-tuple-element.276, pred[]{:T(512)S(6)} %compare.3), kind=kOutput, calls=%fused_computation.8.clone.1 | convolution fusion | flops 136511488 | bytes 5251073 | tf_op jit(solution)/shard_map/while/body/eval_jaxpr/hqk,khd->qhd/dot_general | solution.py:98
  113.2 1.3 constant_dynamic-slice_fusion.2
  115.0 0.8 fusion.70
  115.9 3.5 %fusion.71 = (f32[4,256]{1,0:T(4,128)S(1)}, f32[4,256,1024]{1,2,0:T(8,128)}) fusion(bf16[256,4,32]{0,2,1:T(8,128)(2,1)S(1)} %copy-done.2, bf16[8192,32]{0,1:T(8,128)(2,1)} %get-tuple-element.307, s32[]{:T(128)S(6)} %select_n.14, f32[4,1024,256]{2,1,0:T(8,128)S(1)} %fusion.70), kind=kOutput, calls=%fused_computation.74.clone.1 | convolution fusion | flops 70253568 | bytes 8523780 | tf_op jit(solution)/shard_map/while/body/eval_jaxpr/qhd,kd->hqk/dot_general | solution.py:90
  119.4 3.2 %fusion.75 = f32[256,4,64]{0,2,1:T(8,128)S(1)} fusion(f32[4,256,1024]{1,2,0:T(8,128)} %get-tuple-element.275, f32[4,256]{1,0:T(4,128)S(1)} %get-tuple-element.302, bf16[1024,4,128]{0,2,1:T(8,128)(2,1)S(1)} %bitcast.46, f32[256,4,64]{0,2,1:T(8,128)S(1)} %get-tuple-element.292, f32[256,4]{0,1:T(4,128)S(1)} %get-tuple-element.276, pred[]{:T(512)S(6)} %compare.3), kind=kOutput, calls=%fused_computation.8.clone.1 | convolution fusion | flops 136511488 | bytes 5251073 | tf_op jit(solution)/shard_map/while/body/eval_jaxpr/hqk,khd->qhd/dot_general | solution.py:98
  123.6 1.3 constant_dynamic-slice_fusion.2
  125.5 0.8 fusion.70
  126.3 3.5 %fusion.71 = (f32[4,256]{1,0:T(4,128)S(1)}, f32[4,256,1024]{1,2,0:T(8,128)}) fusion(bf16[256,4,32]{0,2,1:T(8,128)(2,1)S(1)} %copy-done.2, bf16[8192,32]{0,1:T(8,128)(2,1)} %get-tuple-element.307, s32[]{:T(128)S(6)} %select_n.14, f32[4,1024,256]{2,1,0:T(8,128)S(1)} %fusion.70), kind=kOutput, calls=%fused_computation.74.clone.1 | convolution fusion | flops 70253568 | bytes 8523780 | tf_op jit(solution)/shard_map/while/body/eval_jaxpr/qhd,kd->hqk/dot_general | solution.py:90
  129.8 3.2 %fusion.75 = f32[256,4,64]{0,2,1:T(8,128)S(1)} fusion(f32[4,256,1024]{1,2,0:T(8,128)} %get-tuple-element.275, f32[4,256]{1,0:T(4,128)S(1)} %get-tuple-element.302, bf16[1024,4,128]{0,2,1:T(8,128)(2,1)S(1)} %bitcast.46, f32[256,4,64]{0,2,1:T(8,128)S(1)} %get-tuple-element.292, f32[256,4]{0,1:T(4,128)S(1)} %get-tuple-element.276, pred[]{:T(512)S(6)} %compare.3), kind=kOutput, calls=%fused_computation.8.clone.1 | convolution fusion | flops 136511488 | bytes 5251073 | tf_op jit(solution)/shard_map/while/body/eval_jaxpr/hqk,khd->qhd/dot_general | solution.py:98
  134.0 1.3 constant_dynamic-slice_fusion.2
  135.9 0.8 fusion.70
  136.7 3.5 %fusion.71 = (f32[4,256]{1,0:T(4,128)S(1)}, f32[4,256,1024]{1,2,0:T(8,128)}) fusion(bf16[256,4,32]{0,2,1:T(8,128)(2,1)S(1)} %copy-done.2, bf16[8192,32]{0,1:T(8,128)(2,1)} %get-tuple-element.307, s32[]{:T(128)S(6)} %select_n.14, f32[4,1024,256]{2,1,0:T(8,128)S(1)} %fusion.70), kind=kOutput, calls=%fused_computation.74.clone.1 | convolution fusion | flops 70253568 | bytes 8523780 | tf_op jit(solution)/shard_map/while/body/eval_jaxpr/qhd,kd->hqk/dot_general | solution.py:90
  140.3 3.2 %fusion.75 = f32[256,4,64]{0,2,1:T(8,128)S(1)} fusion(f32[4,256,1024]{1,2,0:T(8,128)} %get-tuple-element.275, f32[4,256]{1,0:T(4,128)S(1)} %get-tuple-element.302, bf16[1024,4,128]{0,2,1:T(8,128)(2,1)S(1)} %bitcast.46, f32[256,4,64]{0,2,1:T(8,128)S(1)} %get-tuple-element.292, f32[256,4]{0,1:T(4,128)S(1)} %get-tuple-element.276, pred[]{:T(512)S(6)} %compare.3), kind=kOutput, calls=%fused_computation.8.clone.1 | convolution fusion | flops 136511488 | bytes 5251073 | tf_op jit(solution)/shard_map/while/body/eval_jaxpr/hqk,khd->qhd/dot_general | solution.py:98
  144.5 1.3 constant_dynamic-slice_fusion.2
  146.4 0.8 fusion.70
  147.2 3.5 %fusion.71 = (f32[4,256]{1,0:T(4,128)S(1)}, f32[4,256,1024]{1,2,0:T(8,128)}) fusion(bf16[256,4,32]{0,2,1:T(8,128)(2,1)S(1)} %copy-done.2, bf16[8192,32]{0,1:T(8,128)(2,1)} %get-tuple-element.307, s32[]{:T(128)S(6)} %select_n.14, f32[4,1024,256]{2,1,0:T(8,128)S(1)} %fusion.70), kind=kOutput, calls=%fused_computation.74.clone.1 | convolution fusion | flops 70253568 | bytes 8523780 | tf_op jit(solution)/shard_map/while/body/eval_jaxpr/qhd,kd->hqk/dot_general | solution.py:90
  150.7 3.2 %fusion.75 = f32[256,4,64]{0,2,1:T(8,128)S(1)} fusion(f32[4,256,1024]{1,2,0:T(8,128)} %get-tuple-element.275, f32[4,256]{1,0:T(4,128)S(1)} %get-tuple-element.302, bf16[1024,4,128]{0,2,1:T(8,128)(2,1)S(1)} %bitcast.46, f32[256,4,64]{0,2,1:T(8,128)S(1)} %get-tuple-element.292, f32[256,4]{0,1:T(4,128)S(1)} %get-tuple-element.276, pred[]{:T(512)S(6)} %compare.3), kind=kOutput, calls=%fused_computation.8.clone.1 | convolution fusion | flops 136511488 | bytes 5251073 | tf_op jit(solution)/shard_map/while/body/eval_jaxpr/hqk,khd->qhd/dot_general | solution.py:98
  154.9 1.3 constant_dynamic-slice_fusion.2
  156.8 0.8 fusion.70
  157.6 3.5 %fusion.71 = (f32[4,256]{1,0:T(4,128)S(1)}, f32[4,256,1024]{1,2,0:T(8,128)}) fusion(bf16[256,4,32]{0,2,1:T(8,128)(2,1)S(1)} %copy-done.2, bf16[8192,32]{0,1:T(8,128)(2,1)} %get-tuple-element.307, s32[]{:T(128)S(6)} %select_n.14, f32[4,1024,256]{2,1,0:T(8,128)S(1)} %fusion.70), kind=kOutput, calls=%fused_computation.74.clone.1 | convolution fusion | flops 70253568 | bytes 8523780 | tf_op jit(solution)/shard_map/while/body/eval_jaxpr/qhd,kd->hqk/dot_general | solution.py:90
  161.2 3.2 %fusion.75 = f32[256,4,64]{0,2,1:T(8,128)S(1)} fusion(f32[4,256,1024]{1,2,0:T(8,128)} %get-tuple-element.275, f32[4,256]{1,0:T(4,128)S(1)} %get-tuple-element.302, bf16[1024,4,128]{0,2,1:T(8,128)(2,1)S(1)} %bitcast.46, f32[256,4,64]{0,2,1:T(8,128)S(1)} %get-tuple-element.292, f32[256,4]{0,1:T(4,128)S(1)} %get-tuple-element.276, pred[]{:T(512)S(6)} %compare.3), kind=kOutput, calls=%fused_computation.8.clone.1 | convolution fusion | flops 136511488 | bytes 5251073 | tf_op jit(solution)/shard_map/while/body/eval_jaxpr/hqk,khd->qhd/dot_general | solution.py:98
  165.4 1.3 constant_dynamic-slice_fusion.2
  167.2 0.8 fusion.70
  168.0 3.5 %fusion.71 = (f32[4,256]{1,0:T(4,128)S(1)}, f32[4,256,1024]{1,2,0:T(8,128)}) fusion(bf16[256,4,32]{0,2,1:T(8,128)(2,1)S(1)} %copy-done.2, bf16[8192,32]{0,1:T(8,128)(2,1)} %get-tuple-element.307, s32[]{:T(128)S(6)} %select_n.14, f32[4,1024,256]{2,1,0:T(8,128)S(1)} %fusion.70), kind=kOutput, calls=%fused_computation.74.clone.1 | convolution fusion | flops 70253568 | bytes 8523780 | tf_op jit(solution)/shard_map/while/body/eval_jaxpr/qhd,kd->hqk/dot_general | solution.py:90
  171.6 3.1 %fusion.75 = f32[256,4,64]{0,2,1:T(8,128)S(1)} fusion(f32[4,256,1024]{1,2,0:T(8,128)} %get-tuple-element.275, f32[4,256]{1,0:T(4,128)S(1)} %get-tuple-element.302, bf16[1024,4,128]{0,2,1:T(8,128)(2,1)S(1)} %bitcast.46, f32[256,4,64]{0,2,1:T(8,128)S(1)} %get-tuple-element.292, f32[256,4]{0,1:T(4,128)S(1)} %get-tuple-element.276, pred[]{:T(512)S(6)} %compare.3), kind=kOutput, calls=%fused_computation.8.clone.1 | convolution fusion | flops 136511488 | bytes 5251073 | tf_op jit(solution)/shard_map/while/body/eval_jaxpr/hqk,khd->qhd/dot_general | solution.py:98
  175.6 1.3 constant_dynamic-slice_fusion.2
  177.5 0.8 fusion.70
  178.3 3.5 %fusion.71 = (f32[4,256]{1,0:T(4,128)S(1)}, f32[4,256,1024]{1,2,0:T(8,128)}) fusion(bf16[256,4,32]{0,2,1:T(8,128)(2,1)S(1)} %copy-done.2, bf16[8192,32]{0,1:T(8,128)(2,1)} %get-tuple-element.307, s32[]{:T(128)S(6)} %select_n.14, f32[4,1024,256]{2,1,0:T(8,128)S(1)} %fusion.70), kind=kOutput, calls=%fused_computation.74.clone.1 | convolution fusion | flops 70253568 | bytes 8523780 | tf_op jit(solution)/shard_map/while/body/eval_jaxpr/qhd,kd->hqk/dot_general | solution.py:90
  181.8 3.1 %fusion.75 = f32[256,4,64]{0,2,1:T(8,128)S(1)} fusion(f32[4,256,1024]{1,2,0:T(8,128)} %get-tuple-element.275, f32[4,256]{1,0:T(4,128)S(1)} %get-tuple-element.302, bf16[1024,4,128]{0,2,1:T(8,128)(2,1)S(1)} %bitcast.46, f32[256,4,64]{0,2,1:T(8,128)S(1)} %get-tuple-element.292, f32[256,4]{0,1:T(4,128)S(1)} %get-tuple-element.276, pred[]{:T(512)S(6)} %compare.3), kind=kOutput, calls=%fused_computation.8.clone.1 | convolution fusion | flops 136511488 | bytes 5251073 | tf_op jit(solution)/shard_map/while/body/eval_jaxpr/hqk,khd->qhd/dot_general | solution.py:98
  185.9 1.4 convolution_convert_fusion
  187.4 4.2 %all-to-all-start = ((bf16[4,64,2048]{2,1,0:T(8,128)(2,1)}), bf16[4,64,2048]{2,1,0:T(8,128)(2,1)S(1)}, u32[]{:S(2)}, u32[]{:S(2)}) async-start(bf16[4,64,2048]{2,1,0:T(8,128)(2,1)} %bitcast.3), calls=%async_computation | async-start | bytes 2097152 | tf_op jit(solution)/shard_map/all_to_all | solution.py:19
  191.5 14.8 %all-to-all-done = bf16[4,64,2048]{2,1,0:T(8,128)(2,1)S(1)} async-done(((bf16[4,64,2048]{2,1,0:T(8,128)(2,1)}), bf16[4,64,2048]{2,1,0:T(8,128)(2,1)S(1)}, u32[]{:S(2)}, u32[]{:S(2)}) %all-to-all-start) | async-done | bytes 1048608 | tf_op jit(solution)/shard_map/all_to_all | solution.py:19
  206.5 1.1 fusion.28
  207.8 1.1 broadcast_in_dim.17
  208.9 3.6 %all-to-all-start.1 = ((bf16[4,64,2048]{2,1,0:T(8,128)(2,1)}), bf16[4,64,2048]{2,1,0:T(8,128)(2,1)S(1)}, u32[]{:S(2)}, u32[]{:S(2)}) async-start(bf16[4,64,2048]{2,1,0:T(8,128)(2,1)} %broadcast_in_dim.17), calls=%async_computation.1 | async-start | bytes 2097152 | tf_op jit(solution)/shard_map/all_to_all | solution.py:25
  212.5 41.0 %all-gather.8.cloned.1.call-done = bf16[2048,2048]{0,1:T(8,128)(2,1)} async-done(((bf16[2048,64]{0,1:T(8,128)(2,1)}), bf16[2048,2048]{0,1:T(8,128)(2,1)}) %all-gather.8.cloned.1.call-update) | async-done | bytes 8388624 | tf_op jit(solution)/shard_map/all_gather | solution.py:155
  253.6 10.3 %convolution_convert_fusion.1 = bf16[256,2048]{1,0:T(8,128)(2,1)S(1)} fusion(bf16[2048,2048]{0,1:T(8,128)(2,1)} %all-gather.8.cloned.1.call-done, bf16[256,2048]{1,0:T(8,128)(2,1)S(1)} %bitcast.50, bf16[2048,2048]{1,0:T(8,128)(2,1)} %all-gather.6.cloned.1.call-done), kind=kOutput, calls=%fused_computation.26 | convolution fusion | flops 4297064448 | bytes 18874368 | tf_op jit(solution)/shard_map/dot_general | solution.py:153
  263.8 18.5 %all_to_all.15 = bf16[4,64,2048]{2,1,0:T(8,128)(2,1)S(1)} all-to-all(bf16[4,64,2048]{2,1,0:T(8,128)(2,1)S(1)} %bitcast.51), channel_id=1, replica_groups=mesh['grp'=2,'sp'=32,'tp'=4] {'tp'}, dimensions={0} | all-to-all | bytes 2097152 | tf_op jit(solution)/shard_map/all_to_all | solution.py:19
  (106 shorter events, 17.5 us)
Async XLA Ops:
  6.5 179.4 %copy-start = (bf16[256,2048]{1,0:T(8,128)(2,1)S(1)}, bf16[256,2048]{1,0:T(8,128)(2,1)}, u32[]{:S(2)}) copy-start(bf16[256,2048]{1,0:T(8,128)(2,1)} %param.22) | copy-start | bytes 3145732
  6.6 9.5 %copy-start.3 = (bf16[256,32]{0,1:T(8,128)(2,1)S(1)}, bf16[256,32]{0,1:T(8,128)(2,1)}, u32[]{:S(2)}) copy-start(bf16[256,32]{0,1:T(8,128)(2,1)} %param.17) | copy-start | bytes 49156
  6.6 96.4 %all-gather.4.cloned.1.call-start = ((), (), s32[]{:S(2)}) async-start(), calls=%async_computation.3 | async-start | bytes 8650752 | tf_op jit(solution)/shard_map/all_gather | solution.py:116
  10.0 202.5 %all-gather.6.cloned.1.call-start = ((), (), s32[]{:S(2)}) async-start(), calls=%async_computation.4 | async-start | bytes 8650752 | tf_op jit(solution)/shard_map/all_gather | solution.py:149
  10.8 242.7 %all-gather.8.cloned.1.call-start = ((), (), s32[]{:S(2)}) async-start(), calls=%async_computation.5 | async-start | bytes 8650752 | tf_op jit(solution)/shard_map/all_gather | solution.py:155
  104.8 0.8 copy-start.2
  109.1 3.4 %copy-start.1 = (f32[4,256,1024]{1,2,0:T(8,128)S(1)}, f32[4,256,1024]{1,2,0:T(8,128)}, u32[]{:S(2)}) copy-start(f32[4,256,1024]{1,2,0:T(8,128)} %get-tuple-element.275) | copy-start | bytes 12582916 | tf_op jit(solution)/shard_map/while
  115.0 0.8 copy-start.2
  119.4 3.6 %copy-start.1 = (f32[4,256,1024]{1,2,0:T(8,128)S(1)}, f32[4,256,1024]{1,2,0:T(8,128)}, u32[]{:S(2)}) copy-start(f32[4,256,1024]{1,2,0:T(8,128)} %get-tuple-element.275) | copy-start | bytes 12582916 | tf_op jit(solution)/shard_map/while
  125.5 0.8 copy-start.2
  129.8 3.6 %copy-start.1 = (f32[4,256,1024]{1,2,0:T(8,128)S(1)}, f32[4,256,1024]{1,2,0:T(8,128)}, u32[]{:S(2)}) copy-start(f32[4,256,1024]{1,2,0:T(8,128)} %get-tuple-element.275) | copy-start | bytes 12582916 | tf_op jit(solution)/shard_map/while
  135.9 0.8 copy-start.2
  140.3 3.6 %copy-start.1 = (f32[4,256,1024]{1,2,0:T(8,128)S(1)}, f32[4,256,1024]{1,2,0:T(8,128)}, u32[]{:S(2)}) copy-start(f32[4,256,1024]{1,2,0:T(8,128)} %get-tuple-element.275) | copy-start | bytes 12582916 | tf_op jit(solution)/shard_map/while
  146.3 0.8 copy-start.2
  150.7 3.6 %copy-start.1 = (f32[4,256,1024]{1,2,0:T(8,128)S(1)}, f32[4,256,1024]{1,2,0:T(8,128)}, u32[]{:S(2)}) copy-start(f32[4,256,1024]{1,2,0:T(8,128)} %get-tuple-element.275) | copy-start | bytes 12582916 | tf_op jit(solution)/shard_map/while
  156.8 0.8 copy-start.2
  161.2 3.6 %copy-start.1 = (f32[4,256,1024]{1,2,0:T(8,128)S(1)}, f32[4,256,1024]{1,2,0:T(8,128)}, u32[]{:S(2)}) copy-start(f32[4,256,1024]{1,2,0:T(8,128)} %get-tuple-element.275) | copy-start | bytes 12582916 | tf_op jit(solution)/shard_map/while
  167.2 0.8 copy-start.2
  171.6 3.4 %copy-start.1 = (f32[4,256,1024]{1,2,0:T(8,128)S(1)}, f32[4,256,1024]{1,2,0:T(8,128)}, u32[]{:S(2)}) copy-start(f32[4,256,1024]{1,2,0:T(8,128)} %get-tuple-element.275) | copy-start | bytes 12582916 | tf_op jit(solution)/shard_map/while
  177.5 0.8 copy-start.2
  181.8 3.4 %copy-start.1 = (f32[4,256,1024]{1,2,0:T(8,128)S(1)}, f32[4,256,1024]{1,2,0:T(8,128)}, u32[]{:S(2)}) copy-start(f32[4,256,1024]{1,2,0:T(8,128)} %get-tuple-element.275) | copy-start | bytes 12582916 | tf_op jit(solution)/shard_map/while
  185.9 21.7 %copy-start.4 = (f32[2048]{0:T(1024)S(1)}, f32[2048]{0:T(1024)}, u32[]{:S(2)}) copy-start(f32[2048]{0:T(1024)} %param.23) | copy-start | bytes 24580
  187.4 18.9 %all-to-all-start = ((bf16[4,64,2048]{2,1,0:T(8,128)(2,1)}), bf16[4,64,2048]{2,1,0:T(8,128)(2,1)S(1)}, u32[]{:S(2)}, u32[]{:S(2)}) async-start(bf16[4,64,2048]{2,1,0:T(8,128)(2,1)} %bitcast.3), calls=%async_computation | async-start | bytes 2097152 | tf_op jit(solution)/shard_map/all_to_all | solution.py:19
  208.9 44.7 %all-to-all-start.1 = ((bf16[4,64,2048]{2,1,0:T(8,128)(2,1)}), bf16[4,64,2048]{2,1,0:T(8,128)(2,1)S(1)}, u32[]{:S(2)}, u32[]{:S(2)}) async-start(bf16[4,64,2048]{2,1,0:T(8,128)(2,1)} %broadcast_in_dim.17), calls=%async_computation.1 | async-start | bytes 2097152 | tf_op jit(solution)/shard_map/all_to_all | solution.py:25
Sparse Core Ops, SparseCore 0:
  10.1 92.7 all-gather.3
  104.8 73.3 all-gather.5
  180.1 73.4 all-gather.7
where the time goes:
time: 291 us; the launch traced here: 290 us
  waiting for transfers between devices  88.2 us (30%)
  matrix products  75.2 us (26%)
  blocking collectives  73.7 us (25%)
  local copies, waits for them, and re-layouts  19.8 us (7%)
  between operations  13.3 us (5%)
  other arithmetic  11.1 us (4%)
  starting transfers between devices  7.9 us (3%)
    all_gather x1, blocking collectives, on_device(): lax.all_gather(key_rope, 'sp', axis=0, tiled=True)  55.3 us
    all_gather x1, waiting for transfers between devices, on_device(): lax.all_gather(feed_down, 'sp', axis=1, tiled=True)  41 us
    all_gather x1, waiting for transfers between devices, on_device(): lax.all_gather(own_keys, 'sp', axis=0, tiled=True)  30.9 us
    dot_general x8, matrix products, attend_block(): jnp.einsum('qhd,kd->hqk', query_turned, rope_rows, preferred_element_type...  28.1 us
    dot_general x8, matrix products, attend_block(): jnp.einsum('hqk,khd->qhd', expo.astype(jnp.bfloat16), value_rows, preferr...  25.4 us
    all_to_all x1, blocking collectives, sum_at_owner(): lax.all_to_all(cut_along(value, dim, count), axis, 0, 0, tiled=True)  18.5 us
    all_to_all x1, waiting for transfers between devices, sum_at_owner(): lax.all_to_all(cut_along(value, dim, count), axis, 0, 0, tiled=True)  14.8 us
    dynamic_slice x16, local copies, waits for them, and re-layouts, step_block(): bulk = lax.dynamic_slice_in_dim(pieces[0], first, block, 0)  14.7 us
  transfers between devices with their start and end apart: 5, of which 3 were waited for; matrix products, arithmetic and copies ran while one was open for 30% of the time, Pallas kernels for 0%

commit v1 on v0

--- a/solution.py
+++ b/solution.py
@@ -7,6 +7,14 @@
 QUERY_KEY_PLAIN = 64
 QUERY_KEY_ROTARY = 32
 VALUE_HEAD_SIZE = 64
+
+
+def update_lines_on(u):
+    n_shards = lax.axis_size("sp")
+    xs_all = list(map(lambda it: n_shards if it == 0 else 1, range(u.ndim)))
+    return lax.all_to_all(
+        jnp.tile(u, xs_all), axis_name="sp", split_axis=0, concat_axis=0, tiled=True
+    )
 
 
 def cut_along(value, dim, count):
@@ -112,10 +120,7 @@
     own_keys = jnp.dot(latent, key_value_up_weight, preferred_element_type=jnp.float32).astype(
         jnp.bfloat16
     )
-    pieces = (
-        lax.all_gather(own_keys, "sp", axis=0, tiled=True),
-        lax.all_gather(key_rope, "sp", axis=0, tiled=True),
-    )
+    pieces = (update_lines_on(own_keys), lax.all_gather(key_rope, "sp", axis=0, tiled=True))
     rows_in = pieces[0].shape[0]
     block = math.gcd(rows_in, 1024)
 

time: 291 us -> 673 us (2.31)
  blocking collectives: 73.7 us -> 474 us
  waiting for transfers between devices: 88.2 us -> 29.8 us
  starting transfers between devices: 7.9 us -> 33.8 us
  local copies, waits for them, and re-layouts: 19.8 us -> 35 us
    all_gather x1, blocking collectives: 55.3 us -> 459 us  [on_device(): lax.all_gather(key_rope, 'sp', axis=0, tiled=True)]
    all_gather x1, waiting for transfers between devices: 41 us -> 0.02 us  [on_device(): lax.all_gather(feed_down, 'sp', axis=1, tiled=True)]
    all_gather x1 -> x0, waiting for transfers between devices: 30.9 us -> none  [on_device(): lax.all_gather(own_keys, 'sp', axis=0, tiled=True)]
    all_to_all x0 -> x1, starting transfers between devices: none -> 25.6 us  [update_lines_on(): lax.all_to_all(jnp.tile(u, xs_all), axis_name='sp', split_axis=0, concat_...]
    all_to_all x1, waiting for transfers between devices: 0.01 us -> 13.6 us  [from_everyone(): return lax.all_to_all(copies, axis, split_axis=0, concat_axis=0, tiled=True)]
    all_to_all x0 -> x1, local copies, waits for them, and re-layouts: none -> 12 us  [update_lines_on(): lax.all_to_all(jnp.tile(u, xs_all), axis_name='sp', split_axis=0, concat_...]
  transfers between devices with their start and end apart: 5 -> 5, of which waited for: 3 -> 2; matrix products, arithmetic and copies ran while one was open for 30% -> 14% of each run, Pallas kernels for 0% -> 0%
where the time goes in v1:
time: 673 us; the launch traced here: 669 us
  blocking collectives  474 us (70%)
  matrix products  73.2 us (11%)
  local copies, waits for them, and re-layouts  35 us (5%)
  starting transfers between devices  33.8 us (5%)
  waiting for transfers between devices  29.8 us (4%)
  between operations  13.7 us (2%)
  other arithmetic  9.34 us (1%)
    all_gather x1, blocking collectives, on_device(): lax.all_gather(key_rope, 'sp', axis=0, tiled=True)  459 us
    dot_general x8, matrix products, attend_block(): jnp.einsum('qhd,kd->hqk', query_turned, rope_rows, preferred_element_type...  28.3 us
    all_to_all x1, starting transfers between devices, update_lines_on(): lax.all_to_all(jnp.tile(u, xs_all), axis_name='sp', split_axis=0, concat_...  25.6 us
    dot_general x8, matrix products, attend_block(): jnp.einsum('hqk,khd->qhd', expo.astype(jnp.bfloat16), value_rows, preferr...  25.1 us
    all_to_all x1, blocking collectives, sum_at_owner(): lax.all_to_all(cut_along(value, dim, count), axis, 0, 0, tiled=True)  15.2 us
    all_to_all x1, waiting for transfers between devices, sum_at_owner(): lax.all_to_all(cut_along(value, dim, count), axis, 0, 0, tiled=True)  14.8 us
    dynamic_slice x16, local copies, waits for them, and re-layouts, step_block(): bulk = lax.dynamic_slice_in_dim(pieces[0], first, block, 0)  14.7 us
    all_to_all x1, waiting for transfers between devices, from_everyone(): return lax.all_to_all(copies, axis, split_axis=0, concat_axis=0, tiled=True)  13.6 us
  transfers between devices with their start and end apart: 5, of which 2 were waited for; matrix products, arithmetic and copies ran while one was open for 14% of the time, Pallas kernels for 0%

profile of v1, /device:TPU:33, one launch (start us, length us, event | category | flops | bytes accessed | tf_op | source)
XLA Modules:
  0.0 669.4 jit_solution(5713428881621603947)
XLA Ops:
  6.6 1.2 fusion.25
  7.7 1.5 convolution_convert_fusion.2
  9.4 4.2 tile.2
  13.5 25.6 %all-to-all-start = ((bf16[32,256,512]{1,2,0:T(8,128)(2,1)}), bf16[32,256,512]{1,2,0:T(8,128)(2,1)}, u32[]{:S(2)}, u32[]{:S(2)}) async-start(bf16[32,256,512]{1,2,0:T(8,128)(2,1)} %tile.2), calls=%async_computation | async-start | bytes 16777216 | tf_op jit(solution)/shard_map/all_to_all | solution.py:15
  42.4 458.9 %all_gather.9 = bf16[8192,32]{0,1:T(8,128)(2,1)} all-gather(bf16[256,32]{0,1:T(8,128)(2,1)S(1)} %get-tuple-element.207), channel_id=1, replica_groups=mesh['grp'=2,'sp'=32,'tp'=4] {'sp'}, dimensions={0}, use_global_device_ids=true | all-gather | bytes 540672 | tf_op jit(solution)/shard_map/all_gather | solution.py:123
  501.3 12.0 %copy.27 = bf16[32,256,512]{2,1,0:T(8,128)(2,1)} copy(bf16[32,256,512]{1,2,0:T(8,128)(2,1)} %all-to-all-done) | data formatting | bytes 16777216 | tf_op jit(solution)/shard_map/all_to_all | solution.py:15
  513.3 82.4 %while.18 = (s32[]{:T(128)}, f32[4,256]{1,0:T(4,128)S(1)}, f32[4,256]{1,0:T(4,128)S(1)}, f32[256,4,64]{0,2,1:T(8,128)S(1)}, bf16[8192,512]{1,0:T(8,128)(2,1)}, /...) while((s32[]{:T(128)}, f32[4,256]{1,0:T(4,128)S(1)}, ...), condition=%wide.region_5.0_spmd.clone, body=%wide.region_2.0_spmd.clone.sunk | while | flops 343087104 | bytes 44105964 | solution.py:136
  513.3 1.3 constant_dynamic-slice_fusion.2
  515.1 0.8 fusion.70
  516.0 3.5 fusion.71
  519.5 3.1 fusion.75
  523.6 1.3 constant_dynamic-slice_fusion.2
  525.4 0.8 fusion.70
  526.3 3.5 fusion.71
  529.8 3.1 fusion.75
  533.9 1.3 constant_dynamic-slice_fusion.2
  535.7 0.8 fusion.70
  536.6 3.5 fusion.71
  540.1 3.1 fusion.75
  544.2 1.3 constant_dynamic-slice_fusion.2
  546.0 0.8 fusion.70
  546.9 3.5 fusion.71
  550.4 3.1 fusion.75
  554.5 1.3 constant_dynamic-slice_fusion.2
  556.3 0.8 fusion.70
  557.2 3.5 fusion.71
  560.7 3.1 fusion.75
  564.8 1.3 constant_dynamic-slice_fusion.2
  566.6 0.8 fusion.70
  567.5 3.5 fusion.71
  571.0 3.1 fusion.75
  575.1 1.3 constant_dynamic-slice_fusion.2
  576.9 0.8 fusion.70
  577.8 3.5 fusion.71
  581.3 3.1 fusion.75
  585.4 1.3 constant_dynamic-slice_fusion.2
  587.2 0.8 fusion.70
  588.1 3.5 fusion.71
  591.6 3.1 fusion.75
  595.7 1.4 convolution_convert_fusion
  597.2 4.2 all-to-all-start.1
  601.4 14.8 %all-to-all-done.1 = bf16[4,64,2048]{2,1,0:T(8,128)(2,1)S(1)} async-done(((bf16[4,64,2048]{2,1,0:T(8,128)(2,1)}), bf16[4,64,2048]{2,1,0:T(8,128)(2,1)S(1)}, u32[]{:S(2)}, u32[]{:S(2)}) %all-to-all-start.1) | async-done | bytes 1048608 | tf_op jit(solution)/shard_map/all_to_all | solution.py:27
  616.3 1.1 fusion.28
  617.6 1.1 broadcast_in_dim.17
  618.7 3.8 all-to-all-start.2
  622.6 13.6 %all-to-all-done.2 = bf16[4,64,2048]{2,1,0:T(8,128)(2,1)S(1)} async-done(((bf16[4,64,2048]{2,1,0:T(8,128)(2,1)}), bf16[4,64,2048]{2,1,0:T(8,128)(2,1)S(1)}, u32[]{:S(2)}, u32[]{:S(2)}) %all-to-all-start.2) | async-done | bytes 1048608 | tf_op jit(solution)/shard_map/all_to_all | solution.py:33
  636.1 10.3 %convolution_convert_fusion.1 = bf16[256,2048]{1,0:T(8,128)(2,1)S(1)} fusion(bf16[2048,2048]{0,1:T(8,128)(2,1)} %all-gather.5.cloned.1.call-done, bf16[256,2048]{1,0:T(8,128)(2,1)S(1)} %bitcast.52, bf16[2048,2048]{1,0:T(8,128)(2,1)} %all-gather.3.cloned.1.call-done), kind=kOutput, calls=%fused_computation.26 | convolution fusion | flops 4297064448 | bytes 18874368 | tf_op jit(solution)/shard_map/dot_general | solution.py:158
  646.4 15.2 %all_to_all.24 = bf16[4,64,2048]{2,1,0:T(8,128)(2,1)S(1)} all-to-all(bf16[4,64,2048]{2,1,0:T(8,128)(2,1)S(1)} %bitcast.53), channel_id=1, replica_groups=mesh['grp'=2,'sp'=32,'tp'=4] {'tp'}, dimensions={0} | all-to-all | bytes 2097152 | tf_op jit(solution)/shard_map/all_to_all | solution.py:27
  (114 shorter events, 16.5 us)
Async XLA Ops:
  6.5 589.2 %copy-start = (bf16[256,2048]{1,0:T(8,128)(2,1)S(1)}, bf16[256,2048]{1,0:T(8,128)(2,1)}, u32[]{:S(2)}) copy-start(bf16[256,2048]{1,0:T(8,128)(2,1)} %param.22) | copy-start | bytes 3145732
  13.5 27.2 %copy-start.5 = (bf16[256,32]{0,1:T(8,128)(2,1)S(1)}, bf16[256,32]{0,1:T(8,128)(2,1)}, u32[]{:S(2)}) copy-start(bf16[256,32]{0,1:T(8,128)(2,1)} %param.17) | copy-start | bytes 49156
  13.5 27.3 %copy-start.3 = (bf16[256,768]{1,0:T(8,128)(2,1)S(1)}, bf16[256,768]{1,0:T(8,128)(2,1)}, u32[]{:S(2)}) copy-start(bf16[256,768]{1,0:T(8,128)(2,1)} %param.15) | copy-start | bytes 1179652
  13.5 27.5 %copy-start.4 = (bf16[768,384]{1,0:T(8,128)(2,1)S(1)}, bf16[768,384]{1,0:T(8,128)(2,1)}, u32[]{:S(2)}) copy-start(bf16[768,384]{1,0:T(8,128)(2,1)} %param.20) | copy-start | bytes 1769476
  13.5 27.5 %copy-start.7 = (f32[768]{0:T(1024)S(1)}, f32[768]{0:T(1024)}, u32[]{:S(2)}) copy-start(f32[768]{0:T(1024)} %param.18) | copy-start | bytes 9220
  13.5 487.7 %all-to-all-start = ((bf16[32,256,512]{1,2,0:T(8,128)(2,1)}), bf16[32,256,512]{1,2,0:T(8,128)(2,1)}, u32[]{:S(2)}, u32[]{:S(2)}) async-start(bf16[32,256,512]{1,2,0:T(8,128)(2,1)} %tile.2), calls=%async_computation | async-start | bytes 16777216 | tf_op jit(solution)/shard_map/all_to_all | solution.py:15
  39.2 583.4 %all-gather.3.cloned.1.call-start = ((), (), s32[]{:S(2)}) async-start(), calls=%async_computation.4 | async-start | bytes 8650752 | tf_op jit(solution)/shard_map/all_gather | solution.py:154
  40.0 582.6 %all-gather.5.cloned.1.call-start = ((), (), s32[]{:S(2)}) async-start(), calls=%async_computation.5 | async-start | bytes 8650752 | tf_op jit(solution)/shard_map/all_gather | solution.py:160
  515.1 0.8 copy-start.2
  519.5 3.4 copy-start.1
  525.4 0.8 copy-start.2
  529.8 3.4 copy-start.1
  535.7 0.8 copy-start.2
  540.1 3.4 copy-start.1
  546.0 0.8 copy-start.2
  550.4 3.4 copy-start.1
  556.3 0.8 copy-start.2
  560.7 3.4 copy-start.1
  566.6 0.8 copy-start.2
  571.0 3.4 copy-start.1
  576.9 0.8 copy-start.2
  581.3 3.4 copy-start.1
  587.2 0.8 copy-start.2
  591.6 3.4 copy-start.1
  595.7 21.8 %copy-start.6 = (f32[2048]{0:T(1024)S(1)}, f32[2048]{0:T(1024)}, u32[]{:S(2)}) copy-start(f32[2048]{0:T(1024)} %param.23) | copy-start | bytes 24580
  597.2 19.0 %all-to-all-start.1 = ((bf16[4,64,2048]{2,1,0:T(8,128)(2,1)}), bf16[4,64,2048]{2,1,0:T(8,128)(2,1)S(1)}, u32[]{:S(2)}, u32[]{:S(2)}) async-start(bf16[4,64,2048]{2,1,0:T(8,128)(2,1)} %bitcast.4), calls=%async_computation.1 | async-start | bytes 2097152 | tf_op jit(solution)/shard_map/all_to_all | solution.py:27
  618.7 17.4 %all-to-all-start.2 = ((bf16[4,64,2048]{2,1,0:T(8,128)(2,1)}), bf16[4,64,2048]{2,1,0:T(8,128)(2,1)S(1)}, u32[]{:S(2)}, u32[]{:S(2)}) async-start(bf16[4,64,2048]{2,1,0:T(8,128)(2,1)} %broadcast_in_dim.17), calls=%async_computation.2 | async-start | bytes 2097152 | tf_op jit(solution)/shard_map/all_to_all | solution.py:33
Sparse Core Ops, SparseCore 0:
  41.8 249.9 all-gather.2
  293.6 203.0 all-gather.4
